TPU v7x, 32 devices: a whole 2x2x4 slice. The times are simulated.
32 devices in a mesh: dp: 4 (over y, x), kv: 4 (over z), tp: 2 (over core).
Axes of the slice: x: 2, y: 2, z: 4, core: 2. Of those that a mesh axis runs over, the one named last changes fastest.
Arguments:
- tokens: bfloat16 [4, 3072, 2048], P('dp', 'kv'), may hold values from -60 to 60
- query_weight: bfloat16 [2048, 1024], P(None, 'tp'), may hold values from -0.125 to 0.125
- key_weight: bfloat16 [2048, 256], P(None, 'tp'), may hold values from -0.125 to 0.125
- value_weight: bfloat16 [2048, 256], P(None, 'tp'), may hold values from -0.125 to 0.125
- out_weight: bfloat16 [1024, 2048], P('tp'), may hold values from -3 to 3
- norm_gain: float32 [2048], P('tp'), may hold values from 0.1 to 1.9
- chosen_owner: int32 [4, 24, 4], P('dp'), may hold values from -1 to 3, as said below
- chosen_part: int32 [4, 24, 4], P('dp'), may hold values from 0 to 11, as said below
Outputs:
- attended: bfloat16 [4, 3072, 2048], P('dp', 'kv', 'tp')
Inputs may be any that keep to these rules, and one draw needn't show every extreme that they name: `chosen_owner`: within a row the indices other than -1 are different. Every named key block lies wholly before its query block's first position. Among the 6 rows of one index of kv, no index is named by more than 6 rows. `chosen_part`: 0 where the owner is -1.
All inputs are finite; a program needn't handle non-finite values.
Results may differ from a plain program's by a relative error of at most 0.014.
The roundings to bfloat16 on the way count: a program that leaves them out, or rounds other values in their place, can miss the bound.
Values may be sent and summed in bfloat16 or wider, within the bound.
A program may use at most 128 MiB of HBM per device.

v0:
```python
import jax
import jax.numpy as jnp
from jax import lax
from jax.sharding import PartitionSpec as P

D = 2048
HEAD_DIM = 64
QUERY_BLOCK = 128
KEY_BLOCK = 64
rope_base = 10000.0
norm_eps = 1e-06


def rotate(head_rows, positions):
    half_dim = head_rows.shape[-1] // 2
    frequency = rope_base ** (-jnp.arange(half_dim, dtype=jnp.float32) / half_dim)
    angles = positions.astype(jnp.float32)[:, None] * frequency
    cosine = jnp.cos(angles)[:, None, :]
    sine_part = jnp.sin(angles)[:, None, :]
    first_half = head_rows[..., :half_dim]
    second_half = head_rows[..., half_dim:]
    return jnp.concatenate(
        [
            first_half * cosine - second_half * sine_part,
            second_half * cosine + first_half * sine_part,
        ],
        axis=-1,
    )


def rank_within(flat_ids):
    entry_count = flat_ids.shape[0]
    same_owner = flat_ids[:, None] == flat_ids[None, :]
    earlier = jnp.arange(entry_count)[None, :] < jnp.arange(entry_count)[:, None]
    return jnp.sum(jnp.logical_and(same_owner, earlier), axis=1)


def body(
    tokens, query_weight, key_weight, value_weight, out_weight, norm_gain, chosen_owner, chosen_part
):
    row_data = tokens[0]
    tok_count = row_data.shape[0]
    devices = lax.axis_size("kv")
    my_index = lax.axis_index("kv")
    positions = my_index * tok_count + jnp.arange(tok_count, dtype=jnp.int32)
    heads_here = query_weight.shape[1] // HEAD_DIM
    kv_here = key_weight.shape[1] // HEAD_DIM
    group_size = heads_here // kv_here
    kv_width = kv_here * HEAD_DIM
    queries = rotate(
        jnp.dot(row_data, query_weight, preferred_element_type=jnp.float32).reshape(
            tok_count, heads_here, HEAD_DIM
        ),
        positions,
    ).astype(jnp.bfloat16)
    key_rows = (
        rotate(
            jnp.dot(row_data, key_weight, preferred_element_type=jnp.float32).reshape(
                tok_count, kv_here, HEAD_DIM
            ),
            positions,
        )
        .astype(jnp.bfloat16)
        .reshape(tok_count, kv_width)
    )
    value_rows = jnp.dot(row_data, value_weight, preferred_element_type=jnp.float32).astype(
        jnp.bfloat16
    )
    per_device = tok_count // KEY_BLOCK
    qblocks = tok_count // QUERY_BLOCK
    chosen_count = chosen_owner.shape[2]
    owner_ids = chosen_owner[0]
    part_ids = chosen_part[0]
    mine_owner = lax.dynamic_slice_in_dim(owner_ids, my_index * qblocks, qblocks, 0).reshape(
        qblocks * chosen_count
    )
    mine_valid = mine_owner >= 0
    key_blocks = key_rows.reshape(per_device, KEY_BLOCK, kv_width)
    value_blocks = value_rows.reshape(per_device, KEY_BLOCK, kv_width)
    every_owner = owner_ids.reshape(devices, qblocks * chosen_count)
    every_part = part_ids.reshape(devices, qblocks * chosen_count)
    every_rank = jax.vmap(rank_within)(every_owner)
    slot_ids = jnp.arange(qblocks, dtype=jnp.int32)
    picked_mask = jnp.logical_and(
        (every_owner == my_index)[:, None, :], every_rank[:, None, :] == slot_ids[None, :, None]
    )
    wanted = jnp.sum(jnp.where(picked_mask, every_part[:, None, :], 0), axis=2)
    send_keys = key_blocks[wanted]
    send_values = value_blocks[wanted]
    got_keys, got_values = (
        lax.all_to_all(send_keys, "kv", split_axis=0, concat_axis=0, tiled=True),
        lax.all_to_all(send_values, "kv", split_axis=0, concat_axis=0, tiled=True),
    )
    slot_index = jnp.where(mine_valid, mine_owner * qblocks + rank_within(mine_owner), 0)
    picked_keys = got_keys.reshape(devices * qblocks, KEY_BLOCK, kv_width)[slot_index]
    picked_values = got_values.reshape(devices * qblocks, KEY_BLOCK, kv_width)[slot_index]
    block_queries = queries.reshape(qblocks, QUERY_BLOCK, kv_here, group_size, HEAD_DIM)
    chosen_keys = picked_keys.reshape(qblocks, chosen_count * KEY_BLOCK, kv_here, HEAD_DIM)
    chosen_values = picked_values.reshape(qblocks, chosen_count * KEY_BLOCK, kv_here, HEAD_DIM)
    all_keys = jnp.concatenate(
        [chosen_keys, key_rows.reshape(qblocks, QUERY_BLOCK, kv_here, HEAD_DIM)], axis=1
    )
    all_values = jnp.concatenate(
        [chosen_values, value_rows.reshape(qblocks, QUERY_BLOCK, kv_here, HEAD_DIM)], axis=1
    )
    key_valid = jnp.broadcast_to(
        mine_valid.reshape(qblocks, chosen_count, 1), (qblocks, chosen_count, KEY_BLOCK)
    ).reshape(qblocks, chosen_count * KEY_BLOCK)
    far_mask = jnp.broadcast_to(
        key_valid[:, None, :], (qblocks, QUERY_BLOCK, chosen_count * KEY_BLOCK)
    )
    lower_mask = jnp.broadcast_to(
        (jnp.arange(QUERY_BLOCK)[:, None] >= jnp.arange(QUERY_BLOCK)[None, :])[None],
        (qblocks, QUERY_BLOCK, QUERY_BLOCK),
    )
    full_mask = jnp.concatenate([far_mask, lower_mask], axis=2)
    scores = jnp.einsum(
        "bqngd,bknd->bngqk", block_queries, all_keys, preferred_element_type=jnp.float32
    ) * HEAD_DIM ** (-0.5)
    scores = jnp.where(full_mask[:, None, None], scores, -jnp.inf)
    row_max = jnp.max(scores, axis=-1, keepdims=True)
    weights = jnp.exp(scores - row_max)
    weights = (weights / jnp.sum(weights, axis=-1, keepdims=True)).astype(jnp.bfloat16)
    mixed_rows = (
        jnp.einsum("bngqk,bknd->bqngd", weights, all_values, preferred_element_type=jnp.float32)
        .astype(jnp.bfloat16)
        .reshape(tok_count, heads_here * HEAD_DIM)
    )
    terms = jnp.dot(mixed_rows, out_weight, preferred_element_type=jnp.float32)
    projected = lax.psum_scatter(
        terms.astype(jnp.bfloat16), "tp", scatter_dimension=1, tiled=True
    ).astype(jnp.float32)
    row_total = lax.psum(jnp.sum(projected * projected, axis=1), "tp")
    scale_rows = lax.rsqrt(row_total / D + norm_eps)
    result = (projected * scale_rows[:, None] * norm_gain[None, :]).astype(jnp.bfloat16)
    return result[None]


def solution(mesh):
    placed = (
        P("dp", "kv", None),
        P(None, "tp"),
        P(None, "tp"),
        P(None, "tp"),
        P("tp", None),
        P("tp"),
        P("dp", None, None),
        P("dp", None, None),
    )
    return jax.shard_map(
        body, mesh=mesh, in_specs=placed, out_specs=P("dp", "kv", "tp"), check_vma=False
    )
```

profile of v0, /device:TPU:0, one launch (start us, length us, event | category | flops | bytes accessed | tf_op | source)
XLA Modules:
  0.0 117.1 jit_solution(5359210719336470150)
XLA Ops:
  7.2 2.3 %copy.52 = bf16[2048,128]{0,1:T(8,128)(2,1)} copy(bf16[2048,128]{1,0:T(8,128)(2,1)} %param.10) | data formatting | bytes 1048576 | tf_op args[2]
  9.9 2.2 %fusion.13 = f32[768,2,64]{0,2,1:T(8,128)S(1)} fusion(bf16[2,64,2048]{2,1,0:T(8,128)(2,1)} %bitcast.97, bf16[1,768,2048]{2,1,0:T(8,128)(2,1)S(1)} %copy-done), kind=kOutput, calls=%fused_computation.22 | convolution fusion | flops 402653184 | bytes 4063232 | tf_op jit(solution)/shard_map/dot_general | solution.py:58
  12.9 1.1 copy.53
  14.0 1.2 %convert_element_type.47 = bf16[12,64,128]{2,1,0:T(8,128)(2,1)S(1)} reshape(bf16[768,2,64]{2,1,0:T(2,128)(2,1)} %copy.53) | data formatting | bytes 393216 | tf_op jit(solution)/shard_map/convert_element_type | solution.py:63
  15.9 1.5 %convert_reduce_fusion = s32[4,24]{1,0:T(4,128)} fusion(s32[4,24]{1,0:T(4,128)S(1)} %reshape_squeeze.3, pred[24,24]{1,0:T(8,128)(4,1)} %iota_compare_fusion.2), kind=kLoop, calls=%fused_computation.49 | loop fusion | flops 9120 | bytes 1344 | tf_op jit(solution)/shard_map/vmap()/reduce_sum | solution.py:35
  19.3 1.4 %gather_fusion.2 = bf16[24,64,128]{2,1,0:T(8,128)(2,1)} fusion(bf16[12,64,128]{2,1,0:T(8,128)(2,1)S(1)} %convert_element_type.47, s32[1024]{0:T(1024)S(1)} %pad_clamp_fusion.1), kind=kCustom, calls=%fused_computation.2 | custom fusion | bytes 786528 | tf_op jit(solution)/shard_map/gather | solution.py:88
  20.7 6.3 %all-to-all-start.1 = ((bf16[4,6,64,128]{3,2,1,0:T(8,128)(2,1)}), bf16[4,6,64,128]{3,2,1,0:T(8,128)(2,1)}, u32[]{:S(2)}, u32[]{:S(2)}) async-start(bf16[4,6,64,128]{3,2,1,0:T(8,128)(2,1)} %bitcast.95), calls=%async_computation.1 | async-start | bytes 786432 | tf_op jit(solution)/shard_map/all_to_all | solution.py:91
  28.9 4.0 %copy.57 = bf16[2048,512]{0,1:T(8,128)(2,1)} copy(bf16[2048,512]{1,0:T(8,128)(2,1)} %param.9) | data formatting | bytes 4194304 | tf_op args[1]
  32.9 4.6 %fusion.11 = f32[768,8,64]{0,2,1:T(8,128)} fusion(bf16[8,64,2048]{2,1,0:T(8,128)(2,1)} %bitcast.92, bf16[1,768,2048]{2,1,0:T(8,128)(2,1)S(1)} %copy-done), kind=kOutput, calls=%fused_computation.20 | convolution fusion | flops 1610612736 | bytes 6815744 | tf_op jit(solution)/shard_map/dot_general | solution.py:51
  37.5 1.0 fusion.20
  38.5 1.3 %gather_fusion = bf16[24,64,128]{2,1,0:T(8,128)(2,1)} fusion(bf16[12,64,128]{2,1,0:T(8,128)(2,1)S(1)} %bitcast.93, s32[1024]{0:T(1024)S(1)} %pad_clamp_fusion.1), kind=kCustom, calls=%fused_computation | custom fusion | bytes 786528 | tf_op jit(solution)/shard_map/gather | solution.py:89
  40.6 2.5 %subtract_convert_fusion = (bf16[768,8,32]{0,2,1:T(8,128)(2,1)}, bf16[768,8,32]{0,2,1:T(8,128)(2,1)}) fusion(f32[768,8,64]{0,2,1:T(8,128)} %fusion.11, f32[768,32]{0,1:T(8,128)S(1)} %get-tuple-element.12, f32[768,32]{0,1:T(8,128)S(1)} %get-tuple-element.11), kind=kLoop, calls=%fused_computation.35 | loop fusion | flops 1572864 | bytes 2555904 | tf_op jit(solution)/shard_map/convert.3
  43.0 5.1 %all-to-all-start = ((bf16[4,6,64,128]{3,2,1,0:T(8,128)(2,1)}), bf16[4,6,64,128]{3,2,1,0:T(8,128)(2,1)}, u32[]{:S(2)}, u32[]{:S(2)}) async-start(bf16[4,6,64,128]{3,2,1,0:T(8,128)(2,1)} %bitcast.94), calls=%async_computation | async-start | bytes 786432 | tf_op jit(solution)/shard_map/all_to_all | solution.py:92
  50.0 2.2 %concatenate.37 = bf16[6,128,2,4,32]{1,0,4,3,2:T(8,128)(2,1)} reshape(bf16[768,8,32]{0,2,1:T(8,128)(2,1)} %get-tuple-element.7) | data formatting | bytes 786432 | tf_op jit(solution)/shard_map/concatenate | solution.py:22
  52.2 1.9 %copy.58 = bf16[6,128,2,4,32]{1,4,3,2,0:T(8,128)(2,1)} copy(bf16[6,128,2,4,32]{1,0,4,3,2:T(8,128)(2,1)} %concatenate.37) | data formatting | bytes 786432 | tf_op jit(solution)/shard_map/concatenate | solution.py:22
  54.1 2.2 %concatenate.38 = bf16[6,128,2,4,32]{1,0,4,3,2:T(8,128)(2,1)} reshape(bf16[768,8,32]{0,2,1:T(8,128)(2,1)} %get-tuple-element.8) | data formatting | bytes 786432 | tf_op jit(solution)/shard_map/concatenate | solution.py:22
  56.3 1.9 %copy.59 = bf16[6,128,2,4,32]{1,4,3,2,0:T(8,128)(2,1)} copy(bf16[6,128,2,4,32]{1,0,4,3,2:T(8,128)(2,1)} %concatenate.38) | data formatting | bytes 786432 | tf_op jit(solution)/shard_map/concatenate | solution.py:22
  58.2 0.9 copy.50
  60.2 1.7 %copy_bitcast_fusion = (bf16[6,128,2,32]{1,3,2,0:T(8,128)(2,1)}, bf16[6,128,2,32]{1,3,2,0:T(8,128)(2,1)}) fusion(bf16[768,2,32]{0,2,1:T(8,128)(2,1)} %copy-done.2, bf16[768,2,32]{0,2,1:T(8,128)(2,1)} %copy-done.3), kind=kLoop, calls=%fused_computation.46 | loop fusion | bytes 393216 | tf_op jit(solution)/shard_map/concatenate | solution.py:22
  61.9 1.6 %gather_fusion.3 = bf16[24,64,128]{2,1,0:T(8,128)(2,1)S(1)} fusion(bf16[24,64,128]{2,1,0:T(8,128)(2,1)} %bitcast.14, s32[1024]{0:T(1024)S(1)} %pad_clamp_fusion), kind=kCustom, calls=%fused_computation.3 | custom fusion | bytes 786528 | tf_op jit(solution)/shard_map/gather | solution.py:95
  63.5 1.2 %reshape.208 = bf16[6,256,2,64]{3,2,1,0:T(2,128)(2,1)} reshape(bf16[24,64,128]{2,1,0:T(8,128)(2,1)S(1)} %gather_fusion.3) | data formatting | bytes 786432 | tf_op jit(solution)/shard_map/reshape | solution.py:98
  64.8 2.9 %copy.56 = bf16[6,256,2,64]{1,3,2,0:T(8,128)(2,1)} copy(bf16[6,256,2,64]{3,2,1,0:T(2,128)(2,1)} %reshape.208) | data formatting | bytes 786432 | tf_op jit(solution)/shard_map/reshape | solution.py:98
  67.6 1.6 %gather_fusion.1 = bf16[24,64,128]{2,1,0:T(8,128)(2,1)S(1)} fusion(bf16[24,64,128]{2,1,0:T(8,128)(2,1)} %bitcast.4, s32[1024]{0:T(1024)S(1)} %pad_clamp_fusion), kind=kCustom, calls=%fused_computation.1 | custom fusion | bytes 786528 | tf_op jit(solution)/shard_map/gather | solution.py:96
  69.2 1.2 %reshape.205 = bf16[6,256,2,64]{3,2,1,0:T(2,128)(2,1)} reshape(bf16[24,64,128]{2,1,0:T(8,128)(2,1)S(1)} %gather_fusion.1) | data formatting | bytes 786432 | tf_op jit(solution)/shard_map/reshape | solution.py:99
  70.5 2.2 %copy.49 = bf16[6,256,2,64]{1,3,2,0:T(8,128)(2,1)S(1)} copy(bf16[6,256,2,64]{3,2,1,0:T(2,128)(2,1)} %reshape.205) | data formatting | bytes 786432 | tf_op jit(solution)/shard_map/reshape | solution.py:99
  72.7 8.9 %fusion.38 = (f32[6,2,4,128]{3,2,1,0:T(4,128)}, f32[6,2,4,128,384]{3,4,2,1,0:T(8,128)}) fusion(pred[6,128,384]{1,2,0:T(8,128)(4,1)} %pad_add_fusion, bf16[6,128,2,4,32]{1,4,3,2,0:T(8,128)(2,1)} %copy.59, bf16[6,128,2,4,32]{1,4,3,2,0:T(8,128)(2,1)} %copy.58, bf16[6,128,2,32]{1,3,2,0:T(8,128)(2,1)} %get-tuple-element.15, ...), kind=kOutput, calls=%fused_computation.74 | convolution fusion | flops 314769792 | bytes 11132928 | tf_op jit(solution)/shard_map/sub | solution.py:122
  81.5 4.8 %fusion.19 = bf16[6,128,2,4,64]{1,4,3,2,0:T(8,128)(2,1)S(1)} fusion(f32[6,2,4,128,384]{3,4,2,1,0:T(8,128)} %get-tuple-element.14, f32[6,2,4,128]{3,2,1,0:T(4,128)} %get-tuple-element.13, bf16[6,128,2,64]{1,3,2,0:T(8,128)(2,1)} %copy.50, bf16[6,256,2,64]{1,3,2,0:T(8,128)(2,1)S(1)} %copy.49), kind=kOutput, calls=%fused_computation.28 | convolution fusion | flops 308281344 | bytes 10838016 | tf_op jit(solution)/shard_map/bngqk,bknd->bqngd/dot_general | solution.py:125
  86.9 3.5 %convolution_convert_fusion = bf16[768,2048]{1,0:T(8,128)(2,1)} fusion(bf16[512,2048]{1,0:T(8,128)(2,1)S(1)} %copy-done.7, bf16[64,8,6,128]{3,2,1,0:T(8,128)(2,1)S(1)} %bitcast.96), kind=kOutput, calls=%fused_computation.16 | convolution fusion | flops 1612185600 | bytes 6029312 | tf_op jit(solution)/shard_map/dot_general | solution.py:129
  90.4 12.6 %reduce-scatter.2.cloned.1.call-done = bf16[768,1024]{1,0:T(8,128)(2,1)} async-done(((bf16[768,2048]{1,0:T(8,128)(2,1)}), bf16[768,1024]{1,0:T(8,128)(2,1)}) %reduce-scatter.2.cloned.1.call-update) | async-done | bytes 1572880 | tf_op jit(solution)/shard_map/reduce_scatter | solution.py:130
  103.0 1.8 %fusion.8 = f32[768]{0:T(1024)S(1)} fusion(bf16[768,1024]{1,0:T(8,128)(2,1)} %reduce-scatter.2.cloned.1.call-done), kind=kLoop, calls=%fused_computation.17 | loop fusion | flops 2358528 | bytes 1575936 | tf_op jit(solution)/shard_map/reduce_sum | solution.py:133
  104.8 2.5 %psum.7 = f32[768]{0:T(1024)S(1)} all-reduce(f32[768]{0:T(1024)S(1)} %fusion.8), channel_id=1, replica_groups=mesh['dp'=4,'kv'=4,'tp'=2] {'tp'}, use_global_device_ids=true, to_apply=%region_7.8 | all-reduce | flops 768 | bytes 6144 | tf_op jit(solution)/shard_map/psum | solution.py:133
  107.3 3.0 %fusion.17 = bf16[1,768,1024]{2,1,0:T(8,128)(2,1)} fusion(bf16[768,1024]{1,0:T(8,128)(2,1)} %reduce-scatter.2.cloned.1.call-done, f32[1024]{0:T(1024)S(1)} %copy-done.5, f32[768]{0:T(1024)S(1)} %add_rsqrt_fusion), kind=kLoop, calls=%fused_computation.26 | loop fusion | flops 3145728 | bytes 3152896 | tf_op jit(solution)/shard_map/broadcast_in_dim | solution.py:136
  (60 shorter events, 10.5 us)
Async XLA Ops:
  6.5 3.4 %copy-start = (bf16[1,768,2048]{2,1,0:T(8,128)(2,1)S(1)}, bf16[1,768,2048]{2,1,0:T(8,128)(2,1)}, u32[]{:S(2)}) copy-start(bf16[1,768,2048]{2,1,0:T(8,128)(2,1)} %param.8) | copy-start | bytes 9437188
  9.9 5.3 %copy-start.4 = (s32[1,24,4]{1,2,0:T(4,128)S(1)}, s32[1,24,4]{1,2,0:T(4,128)}, u32[]{:S(2)}) copy-start(s32[1,24,4]{1,2,0:T(4,128)} %param.14) | copy-start | bytes 1156
  12.2 0.6 copy-start.2
  12.2 0.7 copy-start.3
  20.7 22.3 %all-to-all-start.1 = ((bf16[4,6,64,128]{3,2,1,0:T(8,128)(2,1)}), bf16[4,6,64,128]{3,2,1,0:T(8,128)(2,1)}, u32[]{:S(2)}, u32[]{:S(2)}) async-start(bf16[4,6,64,128]{3,2,1,0:T(8,128)(2,1)} %bitcast.95), calls=%async_computation.1 | async-start | bytes 786432 | tf_op jit(solution)/shard_map/all_to_all | solution.py:91
  32.9 4.6 %copy-start.8 = (bf16[2048,128]{1,0:T(8,128)(2,1)S(1)}, bf16[2048,128]{1,0:T(8,128)(2,1)}, u32[]{:S(2)}) copy-start(bf16[2048,128]{1,0:T(8,128)(2,1)} %param.11) | copy-start | bytes 1572868
  40.6 9.2 %copy-start.6 = (pred[6,4]{0,1:T(4,128)(4,1)S(1)}, pred[6,4]{0,1:T(4,128)(4,1)}, u32[]{:S(2)}) copy-start(pred[6,4]{0,1:T(4,128)(4,1)} %fusion.43) | copy-start | bytes 76
  43.0 24.6 %all-to-all-start = ((bf16[4,6,64,128]{3,2,1,0:T(8,128)(2,1)}), bf16[4,6,64,128]{3,2,1,0:T(8,128)(2,1)}, u32[]{:S(2)}, u32[]{:S(2)}) async-start(bf16[4,6,64,128]{3,2,1,0:T(8,128)(2,1)} %bitcast.94), calls=%async_computation | async-start | bytes 786432 | tf_op jit(solution)/shard_map/all_to_all | solution.py:92
  48.1 54.9 %reduce-scatter.2.cloned.1.call-start = ((), (), s32[]{:S(2)}) async-start(), calls=%async_computation.3 | async-start | bytes 4718592 | tf_op jit(solution)/shard_map/reduce_scatter | solution.py:130
  49.7 8.5 %copy-start.1 = (bf16[6,128,2,64]{3,2,1,0:T(2,128)(2,1)S(1)}, bf16[6,128,2,64]{3,2,1,0:T(2,128)(2,1)}, u32[]{:S(2)}) copy-start(bf16[6,128,2,64]{3,2,1,0:T(2,128)(2,1)} %reshape.247) | copy-start | bytes 589828
  81.5 5.4 %copy-start.7 = (bf16[512,2048]{1,0:T(8,128)(2,1)S(1)}, bf16[512,2048]{1,0:T(8,128)(2,1)}, u32[]{:S(2)}) copy-start(bf16[512,2048]{1,0:T(8,128)(2,1)} %param.12) | copy-start | bytes 6291460
  90.4 16.9 %copy-start.5 = (f32[1024]{0:T(1024)S(1)}, f32[1024]{0:T(1024)}, u32[]{:S(2)}) copy-start(f32[1024]{0:T(1024)} %param.13) | copy-start | bytes 12292
Sparse Core Ops, SparseCore 0:
  90.5 12.3 reduce-scatter.1
where the time goes:
time: 118 us; the launch traced here: 117 us
  local copies, waits for them, and re-layouts  37.9 us (32%)
  matrix products  25 us (21%)
  other arithmetic  14.1 us (12%)
  between operations  13.6 us (12%)
  waiting for transfers between devices  12.6 us (11%)
  starting transfers between devices  11.4 us (10%)
  blocking collectives  2.47 us (2%)
    reduce_scatter x1, waiting for transfers between devices, body(): lax.psum_scatter(terms.astype(jnp.bfloat16), 'tp', scatter_dimension=1, t...  12.6 us
    concatenate x6, local copies, waits for them, and re-layouts, rotate(): jnp.concatenate([first_half * cosine - second_half * sine_part, second_ha...  11 us
    sub x1, matrix products, body(): weights = jnp.exp(scores - row_max)  8.85 us
    unnamed x22, local copies, waits for them, and re-layouts  7.87 us
    all_to_all x1, starting transfers between devices, body(): lax.all_to_all(send_keys, 'kv', split_axis=0, concat_axis=0, tiled=True)  6.35 us
    all_to_all x1, starting transfers between devices, body(): lax.all_to_all(send_values, 'kv', split_axis=0, concat_axis=0, tiled=True)  5.1 us
    dot_general x1, matrix products, body(): jnp.einsum('bngqk,bknd->bqngd', weights, all_values, preferred_element_ty...  4.79 us
    dot_general x1, matrix products, body(): jnp.dot(row_data, query_weight, preferred_element_type=jnp.float32)  4.62 us
  transfers between devices with their start and end apart: 3, of which 1 were waited for; matrix products, arithmetic and copies ran while one was open for 30% of the time, Pallas kernels for 0%

commit v1 on v0

--- a/solution.py
+++ b/solution.py
@@ -9,6 +9,22 @@
 KEY_BLOCK = 64
 rope_base = 10000.0
 norm_eps = 1e-06
+
+
+def pairwise_exchange(shard, axis, split, join):
+    ways, here = (lax.axis_size(axis), lax.axis_index(axis))
+    width = shard.shape[split] // ways
+    lengths = list(shard.shape)
+    lengths[split] = width
+    height = lengths[join]
+    lengths[join] = height * ways
+    full = jnp.zeros(lengths, shard.dtype)
+    for mask in range(ways):
+        part = lax.dynamic_slice_in_dim(shard, (here ^ mask) * width, width, axis=split)
+        if mask:
+            part = lax.ppermute(part, axis, [(d, d ^ mask) for d in range(ways)])
+        full = lax.dynamic_update_slice_in_dim(full, part, (here ^ mask) * height, axis=join)
+    return full
 
 
 def rotate(head_rows, positions):
@@ -88,7 +104,7 @@
     send_keys = key_blocks[wanted]
     send_values = value_blocks[wanted]
     got_keys, got_values = (
-        lax.all_to_all(send_keys, "kv", split_axis=0, concat_axis=0, tiled=True),
+        pairwise_exchange(send_keys, "kv", 0, 0),
         lax.all_to_all(send_values, "kv", split_axis=0, concat_axis=0, tiled=True),
     )
     slot_index = jnp.where(mine_valid, mine_owner * qblocks + rank_within(mine_owner), 0)

time: 118 us -> 125 us (1.059)
  local copies, waits for them, and re-layouts: 37.9 us -> 46.4 us
    all_to_all x1 -> x0, starting transfers between devices: 6.35 us -> none  [body(): lax.all_to_all(send_keys, 'kv', split_axis=0, concat_axis=0, tiled=True)]
    ppermute x0 -> x3, starting transfers between devices: none -> 5.82 us  [pairwise_exchange(): part = lax.ppermute(part, axis, [(d, d ^ mask) for d in range(ways)])]
    dynamic_update_slice x0 -> x3, local copies, waits for them, and re-layouts: none -> 4.61 us  [pairwise_exchange(): lax.dynamic_update_slice_in_dim(full, part, (here ^ mask) * height, axis=...]
    concatenate x6, local copies, waits for them, and re-layouts: 11 us -> 9.04 us  [rotate(): jnp.concatenate([first_half * cosine - second_half * sine_part, second_ha...]
    dynamic_slice x0 -> x1, local copies, waits for them, and re-layouts: none -> 1.77 us  [pairwise_exchange(): lax.dynamic_slice_in_dim(shard, (here ^ mask) * width, width, axis=split)]
    another operation x2, other arithmetic: 2.51 us -> 1.01 us
    broadcast_in_dim x2, local copies, waits for them, and re-layouts: 0.36 us -> 1.63 us  [body(): jnp.broadcast_to(key_valid[:, None, :], (qblocks, QUERY_BLOCK, chosen_cou...]
    unnamed x22 -> x24, local copies, waits for them, and re-layouts: 7.87 us -> 7.21 us
  transfers between devices with their start and end apart: 3 -> 5, of which waited for: 1 -> 1; matrix products, arithmetic and copies ran while one was open for 30% -> 41% of each run, Pallas kernels for 0% -> 0%
where the time goes in v1:
time: 125 us; the launch traced here: 124 us
  local copies, waits for them, and re-layouts  46.4 us (37%)
  matrix products  24.7 us (20%)
  between operations  13.6 us (11%)
  other arithmetic  13.2 us (11%)
  waiting for transfers between devices  12.6 us (10%)
  starting transfers between devices  10.7 us (9%)
  blocking collectives  2.48 us (2%)
    reduce_scatter x1, waiting for transfers between devices, body(): lax.psum_scatter(terms.astype(jnp.bfloat16), 'tp', scatter_dimension=1, t...  12.6 us
    concatenate x6, local copies, waits for them, and re-layouts, rotate(): jnp.concatenate([first_half * cosine - second_half * sine_part, second_ha...  9.04 us
    sub x1, matrix products, body(): weights = jnp.exp(scores - row_max)  8.7 us
    unnamed x24, local copies, waits for them, and re-layouts  7.21 us
    ppermute x3, starting transfers between devices, pairwise_exchange(): part = lax.ppermute(part, axis, [(d, d ^ mask) for d in range(ways)])  5.82 us
    all_to_all x1, starting transfers between devices, body(): lax.all_to_all(send_values, 'kv', split_axis=0, concat_axis=0, tiled=True)  4.91 us
    dot_general x1, matrix products, body(): jnp.einsum('bngqk,bknd->bqngd', weights, all_values, preferred_element_ty...  4.8 us
    dynamic_update_slice x3, local copies, waits for them, and re-layouts, pairwise_exchange(): lax.dynamic_update_slice_in_dim(full, part, (here ^ mask) * height, axis=...  4.61 us
  transfers between devices with their start and end apart: 5, of which 1 were waited for; matrix products, arithmetic and copies ran while one was open for 41% of the time, Pallas kernels for 0%

profile of v1, /device:TPU:0, one launch (start us, length us, event | category | flops | bytes accessed | tf_op | source)
XLA Modules:
  0.0 123.7 jit_solution(3685920975023883176)
XLA Ops:
  7.1 2.3 %copy.52 = bf16[2048,128]{0,1:T(8,128)(2,1)} copy(bf16[2048,128]{1,0:T(8,128)(2,1)} %param.10) | data formatting | bytes 1048576 | tf_op args[2]
  9.9 2.3 %fusion.13 = f32[768,2,64]{0,2,1:T(8,128)S(1)} fusion(bf16[2,64,2048]{2,1,0:T(8,128)(2,1)} %bitcast.98, bf16[1,768,2048]{2,1,0:T(8,128)(2,1)S(1)} %copy-done), kind=kOutput, calls=%fused_computation.22 | convolution fusion | flops 402653184 | bytes 4063232 | tf_op jit(solution)/shard_map/dot_general | solution.py:74
  15.4 1.5 %convert_reduce_fusion = s32[4,24]{1,0:T(4,128)} fusion(s32[4,24]{1,0:T(4,128)S(1)} %reshape_squeeze.3, pred[24,24]{1,0:T(8,128)(4,1)} %iota_compare_fusion.2), kind=kLoop, calls=%fused_computation.50 | loop fusion | flops 9120 | bytes 1344 | tf_op jit(solution)/shard_map/vmap()/reduce_sum | solution.py:51
  18.8 1.4 %gather_fusion.2 = bf16[24,64,128]{2,1,0:T(8,128)(2,1)} fusion(bf16[12,64,128]{2,1,0:T(8,128)(2,1)S(1)} %convert_element_type.47, s32[1024]{0:T(1024)S(1)} %pad_clamp_fusion.1), kind=kCustom, calls=%fused_computation.2 | custom fusion | bytes 786528 | tf_op jit(solution)/shard_map/gather | solution.py:104
  20.2 1.8 %constant_dynamic-slice_fusion.3 = (bf16[1,6,64,128]{3,2,1,0:T(8,128)(2,1)}, bf16[1,6,64,128]{3,2,1,0:T(8,128)(2,1)}, bf16[1,6,64,128]{3,2,1,0:T(8,128)(2,1)}, bf16[4,6,64,128]{3,2,1,0:T(8,128)(2,1)S(1)}) fusion(bf16[4,6,64,128]{3,2,1,0:T(8,128)(2,1)} %bitcast.95, s32[]{:T(128)S(6)} %select_n.68, s32[]{:T(128)S(6)} %select_n.67, s32[]{:T(128)S(6)} %select_n.66, ...), kind=kLoop, calls=%fused_computation.68 | loop fusion | bytes 786448 | tf_op jit(solution)/shard_map/dynamic_slice | solution.py:23
  22.0 3.1 %collective-permute-start = (bf16[1,6,64,128]{3,2,1,0:T(8,128)(2,1)}, bf16[1,6,64,128]{3,2,1,0:T(8,128)(2,1)}, u32[]{:S(2)}, u32[]{:S(2)}) collective-permute-start(bf16[1,6,64,128]{3,2,1,0:T(8,128)(2,1)} %get-tuple-element.13), channel_id=1, source_target_pairs={{0,2},{2,0},{4,6},{6,4},{1,3},{3,1},{5,7},{7,5},{8,10},{10,8},{12,... | collective-permute-start | bytes 294920 | tf_op jit(solution)/shard_map/ppermute | solution.py:25
  25.0 2.6 %collective-permute-start.1 = (bf16[1,6,64,128]{3,2,1,0:T(8,128)(2,1)}, bf16[1,6,64,128]{3,2,1,0:T(8,128)(2,1)}, u32[]{:S(2)}, u32[]{:S(2)}) collective-permute-start(bf16[1,6,64,128]{3,2,1,0:T(8,128)(2,1)} %get-tuple-element.12), channel_id=1, source_target_pairs={{0,4},{2,6},{4,0},{6,2},{1,5},{3,7},{5,1},{7,3},{8,12},{10,14},{12... | collective-permute-start | bytes 294920 | tf_op jit(solution)/shard_map/ppermute | solution.py:25
  27.8 2.0 %fusion.20 = bf16[768,128]{1,0:T(8,128)(2,1)S(1)} fusion(bf16[2048,128]{1,0:T(8,128)(2,1)} %param.11, bf16[1,768,2048]{2,1,0:T(8,128)(2,1)S(1)} %copy-done), kind=kOutput, calls=%fused_computation.30 | convolution fusion | flops 402751488 | bytes 3866624 | tf_op jit(solution)/shard_map/dot_general | solution.py:82
  29.8 1.4 %gather_fusion = bf16[24,64,128]{2,1,0:T(8,128)(2,1)} fusion(bf16[12,64,128]{2,1,0:T(8,128)(2,1)S(1)} %bitcast.93, s32[1024]{0:T(1024)S(1)} %pad_clamp_fusion.1), kind=kCustom, calls=%fused_computation | custom fusion | bytes 786528 | tf_op jit(solution)/shard_map/gather | solution.py:105
  31.2 4.9 %all-to-all-start = ((bf16[4,6,64,128]{3,2,1,0:T(8,128)(2,1)}), bf16[4,6,64,128]{3,2,1,0:T(8,128)(2,1)}, u32[]{:S(2)}, u32[]{:S(2)}) async-start(bf16[4,6,64,128]{3,2,1,0:T(8,128)(2,1)} %bitcast.94), calls=%async_computation | async-start | bytes 786432 | tf_op jit(solution)/shard_map/all_to_all | solution.py:108
  44.8 4.0 %copy.57 = bf16[2048,512]{0,1:T(8,128)(2,1)} copy(bf16[2048,512]{1,0:T(8,128)(2,1)} %param.9) | data formatting | bytes 4194304 | tf_op args[1]
  48.8 3.4 %fusion.11 = f32[768,8,64]{0,2,1:T(8,128)S(1)} fusion(bf16[8,64,2048]{2,1,0:T(8,128)(2,1)} %bitcast.92, bf16[1,768,2048]{2,1,0:T(8,128)(2,1)S(1)} %copy-done), kind=kOutput, calls=%fused_computation.20 | convolution fusion | flops 1610612736 | bytes 6815744 | tf_op jit(solution)/shard_map/dot_general | solution.py:67
  53.3 2.2 %concatenate.37 = bf16[6,128,2,4,32]{1,0,4,3,2:T(8,128)(2,1)} reshape(bf16[768,8,32]{0,2,1:T(8,128)(2,1)} %get-tuple-element.7) | data formatting | bytes 786432 | tf_op jit(solution)/shard_map/concatenate | solution.py:38
  55.5 1.9 %copy.58 = bf16[6,128,2,4,32]{1,4,3,2,0:T(8,128)(2,1)} copy(bf16[6,128,2,4,32]{1,0,4,3,2:T(8,128)(2,1)} %concatenate.37) | data formatting | bytes 786432 | tf_op jit(solution)/shard_map/concatenate | solution.py:38
  57.4 1.2 %concatenate.38 = bf16[6,128,2,4,32]{1,0,4,3,2:T(8,128)(2,1)} reshape(bf16[768,8,32]{0,2,1:T(8,128)(2,1)S(1)} %get-tuple-element.8) | data formatting | bytes 786432 | tf_op jit(solution)/shard_map/concatenate | solution.py:38
  58.7 1.9 %copy.59 = bf16[6,128,2,4,32]{1,4,3,2,0:T(8,128)(2,1)} copy(bf16[6,128,2,4,32]{1,0,4,3,2:T(8,128)(2,1)} %concatenate.38) | data formatting | bytes 786432 | tf_op jit(solution)/shard_map/concatenate | solution.py:38
  60.5 1.8 %copy.50 = bf16[6,128,2,64]{1,3,2,0:T(8,128)(2,1)} copy(bf16[6,128,2,64]{3,2,1,0:T(2,128)(2,1)} %reshape.247) | data formatting | bytes 393216 | tf_op jit(solution)/shard_map/reshape | solution.py:120
  64.8 1.5 %constant_dynamic-update-slice_fusion.1 = bf16[4,6,64,128]{3,2,1,0:T(8,128)(2,1)} fusion(bf16[4,6,64,128]{3,2,1,0:T(8,128)(2,1)} %copy-done.1, bf16[1,6,64,128]{3,2,1,0:T(8,128)(2,1)} %collective-permute-done, s32[]{:T(128)S(6)} %select_n.66), kind=kLoop, calls=%fused_computation.64 | loop fusion | bytes 196612 | tf_op jit(solution)/shard_map/dynamic_update_slice | solution.py:26
  66.3 1.5 %constant_dynamic-update-slice_fusion = bf16[4,6,64,128]{3,2,1,0:T(8,128)(2,1)} fusion(bf16[4,6,64,128]{3,2,1,0:T(8,128)(2,1)} %constant_dynamic-update-slice_fusion.1, bf16[1,6,64,128]{3,2,1,0:T(8,128)(2,1)} %collective-permute-done.1, s32[]{:T(128)S(6)} %select_n.67), kind=kLoop, calls=%fused_computation.62 | loop fusion | bytes 196612 | tf_op jit(solution)/shard_map/dynamic_update_slice | solution.py:26
  67.9 1.5 %constant_dynamic-update-slice_fusion.2 = bf16[4,6,64,128]{3,2,1,0:T(8,128)(2,1)} fusion(bf16[4,6,64,128]{3,2,1,0:T(8,128)(2,1)} %constant_dynamic-update-slice_fusion, bf16[1,6,64,128]{3,2,1,0:T(8,128)(2,1)} %collective-permute-done.2, s32[]{:T(128)S(6)} %select_n.68), kind=kLoop, calls=%fused_computation.66 | loop fusion | bytes 196612 | tf_op jit(solution)/shard_map/dynamic_update_slice | solution.py:26
  69.4 1.6 %gather_fusion.3 = bf16[24,64,128]{2,1,0:T(8,128)(2,1)S(1)} fusion(bf16[24,64,128]{2,1,0:T(8,128)(2,1)} %bitcast.96, s32[1024]{0:T(1024)S(1)} %pad_clamp_fusion), kind=kCustom, calls=%fused_computation.3 | custom fusion | bytes 786528 | tf_op jit(solution)/shard_map/gather | solution.py:111
  72.2 2.2 %copy.56 = bf16[6,256,2,64]{1,3,2,0:T(8,128)(2,1)S(1)} copy(bf16[6,256,2,64]{3,2,1,0:T(2,128)(2,1)} %reshape.208) | data formatting | bytes 786432 | tf_op jit(solution)/shard_map/reshape | solution.py:114
  74.4 8.7 %fusion.38 = (f32[6,2,4,128]{3,2,1,0:T(4,128)}, f32[6,2,4,128,384]{3,4,2,1,0:T(8,128)}) fusion(pred[6,128,384]{1,2,0:T(8,128)(4,1)} %pad_add_fusion, bf16[6,128,2,4,32]{1,4,3,2,0:T(8,128)(2,1)} %copy.59, bf16[6,128,2,4,32]{1,4,3,2,0:T(8,128)(2,1)} %copy.58, bf16[6,128,2,32]{1,3,2,0:T(8,128)(2,1)} %get-tuple-element.19, ...), kind=kOutput, calls=%fused_computation.81 | convolution fusion | flops 314769792 | bytes 11132928 | tf_op jit(solution)/shard_map/sub | solution.py:138
  83.1 1.6 %gather_fusion.1 = bf16[24,64,128]{2,1,0:T(8,128)(2,1)S(1)} fusion(bf16[24,64,128]{2,1,0:T(8,128)(2,1)} %bitcast.4, s32[1024]{0:T(1024)S(1)} %pad_clamp_fusion), kind=kCustom, calls=%fused_computation.1 | custom fusion | bytes 786528 | tf_op jit(solution)/shard_map/gather | solution.py:112
  84.8 1.2 reshape.205
  86.0 2.2 %copy.49 = bf16[6,256,2,64]{1,3,2,0:T(8,128)(2,1)S(1)} copy(bf16[6,256,2,64]{3,2,1,0:T(2,128)(2,1)} %reshape.205) | data formatting | bytes 786432 | tf_op jit(solution)/shard_map/reshape | solution.py:115
  88.2 4.8 %fusion.19 = bf16[6,128,2,4,64]{1,4,3,2,0:T(8,128)(2,1)S(1)} fusion(f32[6,2,4,128,384]{3,4,2,1,0:T(8,128)} %get-tuple-element.18, f32[6,2,4,128]{3,2,1,0:T(4,128)} %get-tuple-element.17, bf16[6,128,2,64]{1,3,2,0:T(8,128)(2,1)} %copy.50, bf16[6,256,2,64]{1,3,2,0:T(8,128)(2,1)S(1)} %copy.49), kind=kOutput, calls=%fused_computation.28 | convolution fusion | flops 308281344 | bytes 10838016 | tf_op jit(solution)/shard_map/bngqk,bknd->bqngd/dot_general | solution.py:141
  93.5 3.5 %convolution_convert_fusion = bf16[768,2048]{1,0:T(8,128)(2,1)} fusion(bf16[512,2048]{1,0:T(8,128)(2,1)S(1)} %copy-done.9, bf16[64,8,6,128]{3,2,1,0:T(8,128)(2,1)S(1)} %bitcast.97), kind=kOutput, calls=%fused_computation.16 | convolution fusion | flops 1612185600 | bytes 6029312 | tf_op jit(solution)/shard_map/dot_general | solution.py:145
  97.1 12.6 %reduce-scatter.2.cloned.1.call-done = bf16[768,1024]{1,0:T(8,128)(2,1)} async-done(((bf16[768,2048]{1,0:T(8,128)(2,1)}), bf16[768,1024]{1,0:T(8,128)(2,1)}) %reduce-scatter.2.cloned.1.call-update) | async-done | bytes 1572880 | tf_op jit(solution)/shard_map/reduce_scatter | solution.py:146
  109.6 1.8 %fusion.8 = f32[768]{0:T(1024)S(1)} fusion(bf16[768,1024]{1,0:T(8,128)(2,1)} %reduce-scatter.2.cloned.1.call-done), kind=kLoop, calls=%fused_computation.17 | loop fusion | flops 2358528 | bytes 1575936 | tf_op jit(solution)/shard_map/reduce_sum | solution.py:149
  111.4 2.5 %psum.7 = f32[768]{0:T(1024)S(1)} all-reduce(f32[768]{0:T(1024)S(1)} %fusion.8), channel_id=1, replica_groups=mesh['dp'=4,'kv'=4,'tp'=2] {'tp'}, use_global_device_ids=true, to_apply=%region_7.8 | all-reduce | flops 768 | bytes 6144 | tf_op jit(solution)/shard_map/psum | solution.py:149
  113.9 3.0 %fusion.17 = bf16[1,768,1024]{2,1,0:T(8,128)(2,1)} fusion(bf16[768,1024]{1,0:T(8,128)(2,1)} %reduce-scatter.2.cloned.1.call-done, f32[1024]{0:T(1024)S(1)} %copy-done.8, f32[768]{0:T(1024)S(1)} %add_rsqrt_fusion), kind=kLoop, calls=%fused_computation.26 | loop fusion | flops 3145728 | bytes 3152896 | tf_op jit(solution)/shard_map/broadcast_in_dim | solution.py:152
  (71 shorter events, 20.2 us)
Async XLA Ops:
  6.5 3.4 %copy-start = (bf16[1,768,2048]{2,1,0:T(8,128)(2,1)S(1)}, bf16[1,768,2048]{2,1,0:T(8,128)(2,1)}, u32[]{:S(2)}) copy-start(bf16[1,768,2048]{2,1,0:T(8,128)(2,1)} %param.8) | copy-start | bytes 9437188
  9.9 2.3 %copy-start.2 = (f32[768,32]{0,1:T(8,128)}, f32[768,32]{0,1:T(8,128)S(1)}, u32[]{:S(2)}) copy-start(f32[768,32]{0,1:T(8,128)S(1)} %get-tuple-element.15) | copy-start | bytes 294916
  9.9 2.3 %copy-start.4 = (f32[768,32]{0,1:T(8,128)}, f32[768,32]{0,1:T(8,128)S(1)}, u32[]{:S(2)}) copy-start(f32[768,32]{0,1:T(8,128)S(1)} %get-tuple-element.16) | copy-start | bytes 294916
  9.9 4.7 %copy-start.6 = (s32[1,24,4]{1,2,0:T(4,128)S(1)}, s32[1,24,4]{1,2,0:T(4,128)}, u32[]{:S(2)}) copy-start(s32[1,24,4]{1,2,0:T(4,128)} %param.14) | copy-start | bytes 1156
  22.0 5.6 %copy-start.1 = (bf16[4,6,64,128]{3,2,1,0:T(8,128)(2,1)}, bf16[4,6,64,128]{3,2,1,0:T(8,128)(2,1)S(1)}, u32[]{:S(2)}) copy-start(bf16[4,6,64,128]{3,2,1,0:T(8,128)(2,1)S(1)} %get-tuple-element.14) | copy-start | bytes 1179652
  22.0 42.8 %collective-permute-start = (bf16[1,6,64,128]{3,2,1,0:T(8,128)(2,1)}, bf16[1,6,64,128]{3,2,1,0:T(8,128)(2,1)}, u32[]{:S(2)}, u32[]{:S(2)}) collective-permute-start(bf16[1,6,64,128]{3,2,1,0:T(8,128)(2,1)} %get-tuple-element.13), channel_id=1, source_target_pairs={{0,2},{2,0},{4,6},{6,4},{1,3},{3,1},{5,7},{7,5},{8,10},{10,8},{12,... | collective-permute-start | bytes 294920 | tf_op jit(solution)/shard_map/ppermute | solution.py:25
  25.0 41.3 %collective-permute-start.1 = (bf16[1,6,64,128]{3,2,1,0:T(8,128)(2,1)}, bf16[1,6,64,128]{3,2,1,0:T(8,128)(2,1)}, u32[]{:S(2)}, u32[]{:S(2)}) collective-permute-start(bf16[1,6,64,128]{3,2,1,0:T(8,128)(2,1)} %get-tuple-element.12), channel_id=1, source_target_pairs={{0,4},{2,6},{4,0},{6,2},{1,5},{3,7},{5,1},{7,3},{8,12},{10,14},{12... | collective-permute-start | bytes 294920 | tf_op jit(solution)/shard_map/ppermute | solution.py:25
  27.6 8.5 %copy-start.7 = (s32[1,24,4]{1,2,0:T(4,128)S(1)}, s32[1,24,4]{1,2,0:T(4,128)}, u32[]{:S(2)}) copy-start(s32[1,24,4]{1,2,0:T(4,128)} %param.14) | copy-start | bytes 1156
  27.6 40.2 %collective-permute-start.2 = (bf16[1,6,64,128]{3,2,1,0:T(8,128)(2,1)}, bf16[1,6,64,128]{3,2,1,0:T(8,128)(2,1)}, u32[]{:S(2)}, u32[]{:S(2)}) collective-permute-start(bf16[1,6,64,128]{3,2,1,0:T(8,128)(2,1)} %get-tuple-element.11), channel_id=1, source_target_pairs={{0,6},{2,4},{4,2},{6,0},{1,7},{3,5},{5,3},{7,1},{8,14},{10,12},{12... | collective-permute-start | bytes 294920 | tf_op jit(solution)/shard_map/ppermute | solution.py:25
  31.2 51.9 %all-to-all-start = ((bf16[4,6,64,128]{3,2,1,0:T(8,128)(2,1)}), bf16[4,6,64,128]{3,2,1,0:T(8,128)(2,1)}, u32[]{:S(2)}, u32[]{:S(2)}) async-start(bf16[4,6,64,128]{3,2,1,0:T(8,128)(2,1)} %bitcast.94), calls=%async_computation | async-start | bytes 786432 | tf_op jit(solution)/shard_map/all_to_all | solution.py:108
  36.1 73.5 %reduce-scatter.2.cloned.1.call-start = ((), (), s32[]{:S(2)}) async-start(), calls=%async_computation.2 | async-start | bytes 4718592 | tf_op jit(solution)/shard_map/reduce_scatter | solution.py:146
  48.8 3.5 %copy-start.3 = (f32[768,32]{0,1:T(8,128)S(1)}, f32[768,32]{0,1:T(8,128)}, u32[]{:S(2)}) copy-start(f32[768,32]{0,1:T(8,128)} %copy-done.2) | copy-start | bytes 294916
  48.8 3.5 %copy-start.5 = (f32[768,32]{0,1:T(8,128)S(1)}, f32[768,32]{0,1:T(8,128)}, u32[]{:S(2)}) copy-start(f32[768,32]{0,1:T(8,128)} %copy-done.4) | copy-start | bytes 294916
  88.2 5.4 %copy-start.9 = (bf16[512,2048]{1,0:T(8,128)(2,1)S(1)}, bf16[512,2048]{1,0:T(8,128)(2,1)}, u32[]{:S(2)}) copy-start(bf16[512,2048]{1,0:T(8,128)(2,1)} %param.12) | copy-start | bytes 6291460
  97.0 16.9 %copy-start.8 = (f32[1024]{0:T(1024)S(1)}, f32[1024]{0:T(1024)}, u32[]{:S(2)}) copy-start(f32[1024]{0:T(1024)} %param.13) | copy-start | bytes 12292
Sparse Core Ops, SparseCore 0:
  97.2 12.3 reduce-scatter.1
